TPU v7x, 32 devices: a whole 2x2x4 slice. The times are simulated.
32 devices in a mesh: row: 8 (over z, core), col: 4 (over y, x).
Axes of the slice: x: 2, y: 2, z: 4, core: 2. Of those that a mesh axis runs over, the one named last changes fastest.
Arguments:
- tokens: bfloat16 [4096, 4096], P('row', 'col'), may hold values from -6 to 6
- norm_gain: float32 [4096], replicated, may hold values from 0.1 to 1.9
- out_weight: bfloat16 [4096, 4096], P(None, 'col'), may hold values from -0.09375 to 0.09375
Outputs:
- mixed: bfloat16 [4096, 4096], P('row', 'col')
All inputs are finite; a program needn't handle non-finite values.
Results may differ from a plain program's by a relative error of at most 0.015.
Values may be sent and summed in bfloat16 or wider, within the bound.
A program may use at most 64 MiB of HBM per device.

v0:
```python
import math
import numpy as np
import jax
import jax.numpy as jnp
from jax import lax
from jax.sharding import PartitionSpec as P

GROUPS = 4
EPSILON = 1e-06
PRECISE = lax.Precision.HIGHEST


def phases(left_idx, right_idx, period):
    product = left_idx[:, None] * right_idx[None, :] % period
    angles = product.astype(jnp.float32) * (2.0 * math.pi / period)
    return (jnp.cos(angles), jnp.sin(angles))


def split_table(table):
    table_high = table.astype(jnp.bfloat16)
    remainder = table - table_high.astype(jnp.float32)
    table_middle = remainder.astype(jnp.bfloat16)
    table_low = (remainder - table_middle.astype(jnp.float32)).astype(jnp.bfloat16)
    return (table_high, table_middle, table_low)


def host_tables(group_len, row_count, block_len):
    seq_len = block_len * row_count
    half = group_len // 2 // row_count
    slot = np.arange(group_len)
    freq = slot // (2 * half) * half + slot % half
    odd = slot // half % 2 == 1
    nyquist = odd & (freq == 0)
    sine = odd & ~nyquist
    freq = np.where(nyquist, group_len // 2, freq)
    chan = np.arange(group_len)
    angle = 2 * np.pi * (chan[:, None] * freq[None, :] % group_len) / group_len
    chan_table = np.where(sine[None, :], np.sin(angle), np.cos(angle)) / np.sqrt(group_len)
    low = np.arange(block_len)
    angle = 2 * np.pi * (low[:, None] * low[None, :] % block_len) / block_len
    low_table = np.concatenate([np.cos(angle), np.sin(angle)], 1) / np.sqrt(seq_len)
    high = np.arange(row_count)
    angle = 2 * np.pi * (high[:, None] * low[None, :] % seq_len) / seq_len
    return (chan_table, low_table, np.cos(angle), np.sin(angle))


def slot_facts(slot, group_len, row_count):
    half = group_len // 2 // row_count
    freq = slot // (2 * half) * half + slot % half
    odd = slot // half % 2 == 1
    nyquist = odd & (freq == 0)
    return (jnp.where(nyquist, group_len // 2, freq), odd & ~nyquist)


def folding(group_len, row_count):
    freq, sine = slot_facts(jnp.arange(group_len, dtype=jnp.int32), group_len, row_count)
    chan = jnp.arange(group_len, dtype=jnp.int32)[None, :]
    direct = chan == freq[:, None]
    mirror = chan == ((group_len - freq) % group_len)[:, None]
    signed = jnp.where(sine[:, None], -1.0, 1.0)
    return jnp.where(direct, signed, jnp.where(mirror, 1.0, 0.0)).astype(jnp.bfloat16)


def on_device_folded(tokens, norm_gain, out_weight):
    row_count = lax.axis_size("row")
    col_count = lax.axis_size("col")
    block_len, group_len = tokens.shape
    full_width = group_len * col_count
    slab = group_len // row_count
    out_width = out_weight.shape[1]
    chan_table, low_table, twist_cos, twist_sin = host_tables(group_len, row_count, block_len)
    chan_table = jnp.asarray(chan_table, jnp.bfloat16)
    low_table = jnp.asarray(low_table, jnp.bfloat16)
    twist_cos = jnp.asarray(twist_cos, jnp.float32)[:, :, None]
    twist_sin = jnp.asarray(twist_sin, jnp.float32)[:, :, None]
    values = tokens.astype(jnp.float32)
    total = lax.psum(jnp.sum(values * values, axis=-1), "col")
    inv_rms = lax.rsqrt(total / full_width + EPSILON)[:, None]
    gain = lax.dynamic_slice_in_dim(norm_gain, lax.axis_index("col") * group_len, group_len)
    normed = (values * inv_rms * gain).astype(jnp.bfloat16)
    chans = jnp.dot(normed, chan_table, preferred_element_type=jnp.float32).astype(jnp.bfloat16)
    moved = lax.all_to_all(chans, "row", split_axis=1, concat_axis=0, tiled=True)
    blocks = moved.reshape(row_count, block_len, slab).astype(jnp.float32)
    _, sine = slot_facts(
        lax.axis_index("row") * slab + jnp.arange(slab, dtype=jnp.int32), group_len, row_count
    )
    tops, bottoms = ([], [])
    for q in range(row_count):
        real, imag = (0.0, 0.0)
        for a in range(row_count):
            angle = 2 * math.pi * (a * q % row_count) / row_count
            real = real + blocks[a] * round(math.cos(angle), 12)
            imag = imag - blocks[a] * round(math.sin(angle), 12)
        turned_real = real * twist_cos[q] + imag * twist_sin[q]
        turned_imag = imag * twist_cos[q] - real * twist_sin[q]
        tops.append(jnp.where(sine, -turned_imag, turned_real).astype(jnp.bfloat16))
        bottoms.append(jnp.where(sine, turned_real, turned_imag).astype(jnp.bfloat16))
    stacked = jnp.concatenate([jnp.concatenate(tops, 1), jnp.concatenate(bottoms, 1)], 0)
    lows = jnp.dot(low_table, stacked, preferred_element_type=jnp.float32).astype(jnp.bfloat16)
    back = lax.all_to_all(
        lows.reshape(row_count, block_len // row_count, row_count * slab),
        "row",
        split_axis=0,
        concat_axis=0,
        tiled=True,
    )
    gathered = lax.all_gather(back, "col", axis=0, tiled=False)
    fold = folding(group_len, row_count)
    folded = jnp.einsum(
        "sm,gme->gse",
        fold,
        out_weight.reshape(col_count, group_len, out_width),
        preferred_element_type=jnp.float32,
    ).astype(jnp.bfloat16)
    mapped = jnp.einsum(
        "gspql,gsle->pqe",
        gathered.reshape(col_count, row_count, block_len // row_count, row_count, slab),
        folded.reshape(col_count, row_count, slab, out_width),
        preferred_element_type=jnp.float32,
    )
    return mapped.astype(jnp.bfloat16).reshape(block_len, out_width)


def on_device(tokens, norm_gain, out_weight):
    row_count = lax.axis_size("row")
    col_count = lax.axis_size("col")
    block_len, local_width = tokens.shape
    full_width = local_width * col_count
    group_len = full_width // GROUPS
    share_len = block_len // col_count
    seq_len = block_len * row_count
    slab_len = full_width // row_count
    col_index = lax.axis_index("col")
    chan_idx = jnp.arange(group_len, dtype=jnp.int32)
    cosines, sines = phases(chan_idx, chan_idx, group_len)
    chan_table = jnp.concatenate([cosines, sines], axis=1) / math.sqrt(group_len)
    table_parts = split_table(chan_table)
    arranged = tokens.reshape(col_count, share_len, local_width)
    portion = lax.all_to_all(arranged, "col", split_axis=0, concat_axis=2, tiled=True)
    item_count = portion.shape[1]
    values = portion.astype(jnp.float32)
    inv_rms = lax.rsqrt(jnp.mean(values * values, axis=-1, keepdims=True) + EPSILON)
    normed = lax.optimization_barrier((values * inv_rms * norm_gain).astype(jnp.bfloat16))
    grouped = normed.reshape(item_count, GROUPS, group_len)
    result = jnp.einsum("pgm,mj->pgj", grouped, table_parts[0], preferred_element_type=jnp.float32)
    result = result + jnp.einsum(
        "pgm,mj->pgj", grouped, table_parts[1], preferred_element_type=jnp.float32
    )
    result = result + jnp.einsum(
        "pgm,mj->pgj", grouped, table_parts[2], preferred_element_type=jnp.float32
    )
    high_idx = jnp.arange(row_count, dtype=jnp.int32)
    high_cos, high_sin = phases(high_idx, high_idx, row_count)
    high_table = jnp.concatenate(
        [jnp.concatenate([high_cos, -high_sin], 1), jnp.concatenate([-high_sin, -high_cos], 1)], 0
    )
    parts = (
        lax.all_to_all(
            result[..., :group_len].reshape(1, item_count, full_width),
            "row",
            split_axis=2,
            concat_axis=0,
            tiled=True,
        ),
        lax.all_to_all(
            result[..., group_len:].reshape(1, item_count, full_width),
            "row",
            split_axis=2,
            concat_axis=0,
            tiled=True,
        ),
    )
    item_count = parts[0].shape[1]
    stacked = jnp.concatenate(parts, 0).reshape(2 * row_count, item_count * slab_len)
    result = jnp.dot(high_table, stacked, precision=PRECISE)
    real_part = result[:row_count].reshape(row_count, item_count, slab_len)
    imag_part = result[row_count:].reshape(row_count, item_count, slab_len)
    local_pos = col_index * share_len + jnp.arange(share_len, dtype=jnp.int32)
    twist_cos, twist_sin = phases(high_idx, local_pos, seq_len)
    twist_cos = twist_cos[:, :, None]
    twist_sin = twist_sin[:, :, None]
    turned_real = real_part * twist_cos + imag_part * twist_sin
    turned_imag = imag_part * twist_cos - real_part * twist_sin
    low_idx = jnp.arange(block_len, dtype=jnp.int32)
    low_cos, low_sin = phases(low_idx, low_idx, block_len)
    low_cos = low_cos / math.sqrt(seq_len)
    low_sin = low_sin / math.sqrt(seq_len)
    low_table = jnp.concatenate([low_cos, low_sin], 1)
    stacked = jnp.concatenate(
        (
            lax.all_to_all(turned_real, "col", split_axis=0, concat_axis=1, tiled=True),
            lax.all_to_all(turned_imag, "col", split_axis=0, concat_axis=1, tiled=True),
        ),
        1,
    )
    finished = (jnp.einsum("ks,asc->akc", low_table, stacked, precision=PRECISE),)[0]
    spectrum = finished.astype(jnp.bfloat16)
    returned = lax.all_to_all(spectrum, "row", split_axis=1, concat_axis=2, tiled=True)
    mapped = jnp.einsum(
        "akd,de->kae",
        lax.all_gather(returned, "col", axis=0, tiled=True),
        out_weight,
        preferred_element_type=jnp.float32,
    )
    return mapped.astype(jnp.bfloat16).reshape(block_len, local_width)


def solution(mesh):

    def body(tokens, norm_gain, out_weight):
        whole_groups = tokens.shape[1] * GROUPS == out_weight.shape[0]
        program = on_device_folded if whole_groups else on_device
        return program(tokens, norm_gain, out_weight)

    placed = (P("row", "col"), P(), P(None, "col"))
    return jax.shard_map(
        body, mesh=mesh, in_specs=placed, out_specs=P("row", "col"), check_vma=False
    )
```

profile of v0, /device:TPU:0, one launch (start us, length us, event | category | flops | bytes accessed | tf_op | source)
XLA Modules:
  0.0 159.7 jit_solution(6261747024273125081)
XLA Ops:
  6.5 1.5 fusion
  8.0 11.4 %psum.7 = f32[512]{0:T(512)S(1)} all-reduce(f32[512]{0:T(512)S(1)} %fusion), channel_id=1, replica_groups=mesh['row'=8,'col'=4] {'col'}, use_global_device_ids=true, to_apply=%region_1.0 | all-reduce | flops 512 | bytes 4096 | tf_op jit(solution)/shard_map/psum | solution.py:77
  19.4 0.7 dynamic_slice.3
  20.1 3.2 %fusion.10 = bf16[64,8,8,128]{3,2,1,0:T(8,128)(2,1)S(1)} fusion(bf16[1024,1024]{1,0:T(8,128)(2,1)} %constant.151.clone, bf16[512,1024]{1,0:T(8,128)(2,1)} %param.7, f32[1024]{0:T(1024)S(1)} %dynamic_slice.3, f32[512]{0:T(512)S(1)} %add_rsqrt_fusion), kind=kOutput, calls=%fused_computation.19 | convolution fusion | flops 1076363264 | bytes 4200448 | tf_op jit(solution)/shard_map/dot_general | solution.py:81
  23.4 1.2 copy.26
  24.5 4.9 %all-to-all-start = ((bf16[512,8,128]{2,0,1:T(8,128)(2,1)}), bf16[512,8,128]{2,0,1:T(8,128)(2,1)S(1)}, u32[]{:S(2)}, u32[]{:S(2)}) async-start(bf16[512,8,128]{2,0,1:T(8,128)(2,1)} %bitcast.434), calls=%async_computation | async-start | bytes 2097152 | tf_op jit(solution)/shard_map/all_to_all | solution.py:82
  29.4 0.0 all-gather.3.cloned.1.call-start
  29.5 26.5 %all-to-all-done = bf16[512,8,128]{2,0,1:T(8,128)(2,1)S(1)} async-done(((bf16[512,8,128]{2,0,1:T(8,128)(2,1)}), bf16[512,8,128]{2,0,1:T(8,128)(2,1)S(1)}, u32[]{:S(2)}, u32[]{:S(2)}) %all-to-all-start) | async-done | bytes 1048608 | tf_op jit(solution)/shard_map/all_to_all | solution.py:82
  56.0 0.1 convert_bitcast_fusion
  56.1 0.0 copy-start.14
  56.1 0.0 copy-start.15
  56.1 0.0 copy-start.8
  56.1 0.0 copy-start.9
  56.1 0.3 fusion.23
  56.4 0.4 copy-done.14
  56.8 0.0 copy-done.15
  56.8 0.0 copy-start.6
  56.8 0.0 copy-start.7
  56.8 0.4 fusion.24
  57.2 0.0 copy-done.8
  57.2 0.0 copy-done.9
  57.2 0.0 copy-start.12
  57.2 0.0 copy-start.13
  57.2 0.4 fusion.25
  57.6 0.0 copy-done.6
  57.6 0.0 copy-done.7
  57.7 0.4 fusion.26
  58.1 0.0 copy-start.4
  58.1 0.0 copy-start.5
  58.1 0.0 copy-done.12
  58.1 0.0 copy-done.13
  58.1 0.3 fusion.27
  58.4 0.0 copy-start.2
  58.4 0.0 copy-start.3
  58.4 0.3 copy-done.4
  58.7 0.0 copy-done.5
  58.8 0.0 copy-start.10
  58.8 0.0 copy-start.11
  58.8 0.4 fusion.28
  59.2 0.0 copy-done.2
  59.2 0.0 copy-done.3
  59.2 0.4 fusion.29
  59.6 0.0 copy-done.10
  59.6 0.0 copy-done.11
  59.6 0.5 fusion.30
  60.1 0.0 copy-start.1
  60.1 0.3 fusion.17
  60.4 0.3 fusion.18
  60.6 0.3 fusion.19
  60.9 0.3 fusion.20
  61.2 0.3 fusion.21
  61.4 0.0 copy-start
  61.5 0.3 fusion.22
  61.7 0.0 copy-done.1
  61.7 0.7 fusion.50
  62.5 0.0 copy-done
  62.5 0.7 add_convert_fusion
  63.2 29.7 %all_to_all.18 = bf16[8,64,1024]{2,1,0:T(8,128)(2,1)} all-to-all(bf16[8,64,1024]{2,1,0:T(8,128)(2,1)S(1)} %bitcast.437), channel_id=1, replica_groups=mesh['row'=8,'col'=4] {'row'}, dimensions={0} | all-to-all | bytes 2097152 | tf_op jit(solution)/shard_map/all_to_all | solution.py:100
  92.9 0.0 all-gather.3.cloned.1.call-update
  93.0 14.8 %convolution_convert_fusion = bf16[1024,4,1024]{2,0,1:T(8,128)(2,1)} fusion(bf16[4,1024,1024]{2,1,0:T(8,128)(2,1)} %bitcast.438, s32[1024]{0:T(1024)S(1)} %get-tuple-element.30, bf16[1024]{0:T(1024)(128)(2,1)S(1)} %and_select_fusion, s32[1024]{0:T(1024)S(1)} %get-tuple-element.31), kind=kOutput, calls=%fused_computation | convolution fusion | flops 8598323200 | bytes 16787456 | tf_op jit(solution)/shard_map/sm,gme->gse/dot_general | solution.py:109
  107.7 35.0 %all-gather.3.cloned.1.call-done = bf16[32,64,1024]{2,1,0:T(8,128)(2,1)} async-done(((bf16[8,64,1024]{2,1,0:T(8,128)(2,1)}), bf16[32,64,1024]{2,1,0:T(8,128)(2,1)}) %all-gather.3.cloned.1.call-update) | async-done | bytes 4194320 | tf_op jit(solution)/shard_map/all_gather | solution.py:107
  142.7 3.5 %copy.24 = bf16[256,8,8,128]{3,2,1,0:T(8,128)(2,1)S(1)} copy(bf16[256,8,8,128]{3,1,2,0:T(8,128)(2,1)} %bitcast.435) | data formatting | bytes 8388608
  146.2 1.1 copy-done.16
  147.3 5.5 %fusion.11 = bf16[512,1024]{1,0:T(8,128)(2,1)} fusion(bf16[4,8,64,8,128]{4,3,2,1,0:T(8,128)(2,1)S(1)} %bitcast.436, bf16[4,8,128,1024,1]{3,2,4,1,0:T(8,128)(2,1)S(1)} %bitcast.439), kind=kOutput, calls=%fused_computation.20 | convolution fusion | flops 4295491584 | bytes 13631488 | tf_op jit(solution)/shard_map/gspql,gsle->pqe/dot_general | solution.py:115
  (5 shorter events, 0.1 us)
Async XLA Ops:
  24.5 31.4 %all-to-all-start = ((bf16[512,8,128]{2,0,1:T(8,128)(2,1)}), bf16[512,8,128]{2,0,1:T(8,128)(2,1)S(1)}, u32[]{:S(2)}, u32[]{:S(2)}) async-start(bf16[512,8,128]{2,0,1:T(8,128)(2,1)} %bitcast.434), calls=%async_computation | async-start | bytes 2097152 | tf_op jit(solution)/shard_map/all_to_all | solution.py:82
  29.4 113.3 %all-gather.3.cloned.1.call-start = ((), (), s32[]{:S(2)}) async-start(), calls=%async_computation.2 | async-start | bytes 5242880 | tf_op jit(solution)/shard_map/all_gather | solution.py:107
  56.1 0.7 copy-start.14
  56.1 0.7 copy-start.15
  56.1 1.1 copy-start.8
  56.1 1.1 copy-start.9
  56.8 0.8 copy-start.6
  56.8 0.8 copy-start.7
  57.2 0.9 copy-start.12
  57.2 0.9 copy-start.13
  58.1 0.7 copy-start.4
  58.1 0.7 copy-start.5
  58.4 0.8 copy-start.2
  58.4 0.8 copy-start.3
  58.8 0.8 copy-start.10
  58.8 0.8 copy-start.11
  60.1 1.6 %copy-start.1 = (bf16[512,512]{1,0:T(8,128)(2,1)S(1)}, bf16[512,512]{1,0:T(8,128)(2,1)}, u32[]{:S(2)}) copy-start(bf16[512,512]{1,0:T(8,128)(2,1)} %constant.187) | copy-start | bytes 1572868
  61.4 1.0 copy-start
  142.7 4.6 %copy-start.16 = (bf16[1024,4,1024]{2,0,1:T(8,128)(2,1)S(1)}, bf16[1024,4,1024]{2,0,1:T(8,128)(2,1)}, u32[]{:S(2)}) copy-start(bf16[1024,4,1024]{2,0,1:T(8,128)(2,1)} %convolution_convert_fusion) | copy-start | bytes 25165828
Sparse Core Ops, SparseCore 0:
  93.0 49.6 all-gather.2
where the time goes:
time: 160 us
  waiting for transfers between devices  61.5 us (38%)
  blocking collectives  41.1 us (26%)
  matrix products  24.9 us (16%)
  between operations  13.7 us (9%)
  local copies, waits for them, and re-layouts  7.33 us (5%)
  other arithmetic  6.34 us (4%)
  starting transfers between devices  4.91 us (3%)
    all_gather x1, waiting for transfers between devices, on_device_folded(): gathered = lax.all_gather(back, 'col', axis=0, tiled=False)  35 us
    all_to_all x1, blocking collectives, on_device_folded(): lax.all_to_all(lows.reshape(row_count, block_len // row_count, row_count...  29.7 us
    all_to_all x1, waiting for transfers between devices, on_device_folded(): lax.all_to_all(chans, 'row', split_axis=1, concat_axis=0, tiled=True)  26.5 us
    dot_general x1, matrix products, on_device_folded(): jnp.einsum('sm,gme->gse', fold, out_weight.reshape(col_count, group_len,...  14.8 us
    psum x1, blocking collectives, on_device_folded(): total = lax.psum(jnp.sum(values * values, axis=-1), 'col')  11.4 us
    dot_general x1, matrix products, on_device_folded(): jnp.einsum('gspql,gsle->pqe', gathered.reshape(col_count, row_count, bloc...  5.52 us
    unnamed x35, local copies, waits for them, and re-layouts  5.47 us
    all_to_all x1, starting transfers between devices, on_device_folded(): lax.all_to_all(chans, 'row', split_axis=1, concat_axis=0, tiled=True)  4.87 us
  transfers between devices with their start and end apart: 2, of which 2 were waited for; matrix products, arithmetic and copies ran while one was open for 9% of the time, Pallas kernels for 0%

commit v1 on v0

--- a/solution.py
+++ b/solution.py
@@ -74,7 +74,7 @@
     twist_cos = jnp.asarray(twist_cos, jnp.float32)[:, :, None]
     twist_sin = jnp.asarray(twist_sin, jnp.float32)[:, :, None]
     values = tokens.astype(jnp.float32)
-    total = lax.psum(jnp.sum(values * values, axis=-1), "col")
+    total = jnp.sum(lax.all_gather(jnp.sum(values * values, axis=-1), "col"), axis=0)
     inv_rms = lax.rsqrt(total / full_width + EPSILON)[:, None]
     gain = lax.dynamic_slice_in_dim(norm_gain, lax.axis_index("col") * group_len, group_len)
     normed = (values * inv_rms * gain).astype(jnp.bfloat16)

time: 160 us -> 159 us (level)
  blocking collectives: 41.1 us -> 39.3 us
    psum x1 -> x0, blocking collectives: 11.4 us -> none  [on_device_folded(): total = lax.psum(jnp.sum(values * values, axis=-1), 'col')]
    all_gather x0 -> x1, blocking collectives: none -> 9.57 us  [on_device_folded(): lax.all_gather(jnp.sum(values * values, axis=-1), 'col')]
where the time goes in v1:
time: 159 us
  waiting for transfers between devices  62.4 us (39%)
  blocking collectives  39.3 us (25%)
  matrix products  24.9 us (16%)
  between operations  13.7 us (9%)
  local copies, waits for them, and re-layouts  7.33 us (5%)
  other arithmetic  6.36 us (4%)
  starting transfers between devices  4.93 us (3%)
    all_gather x1, waiting for transfers between devices, on_device_folded(): gathered = lax.all_gather(back, 'col', axis=0, tiled=False)  35.9 us
    all_to_all x1, blocking collectives, on_device_folded(): lax.all_to_all(lows.reshape(row_count, block_len // row_count, row_count...  29.7 us
    all_to_all x1, waiting for transfers between devices, on_device_folded(): lax.all_to_all(chans, 'row', split_axis=1, concat_axis=0, tiled=True)  26.5 us
    dot_general x1, matrix products, on_device_folded(): jnp.einsum('sm,gme->gse', fold, out_weight.reshape(col_count, group_len,...  14.8 us
    all_gather x1, blocking collectives, on_device_folded(): lax.all_gather(jnp.sum(values * values, axis=-1), 'col')  9.57 us
    dot_general x1, matrix products, on_device_folded(): jnp.einsum('gspql,gsle->pqe', gathered.reshape(col_count, row_count, bloc...  5.52 us
    unnamed x35, local copies, waits for them, and re-layouts  5.47 us
    all_to_all x1, starting transfers between devices, on_device_folded(): lax.all_to_all(chans, 'row', split_axis=1, concat_axis=0, tiled=True)  4.89 us
  transfers between devices with their start and end apart: 2, of which 2 were waited for; matrix products, arithmetic and copies ran while one was open for 9% of the time, Pallas kernels for 0%

profile of v1, /device:TPU:0, one launch (start us, length us, event | category | flops | bytes accessed | tf_op | source)
XLA Modules:
  0.0 158.9 jit_solution(18290271655385250812)
XLA Ops:
  6.5 1.5 fusion
  8.0 9.6 %all-gather.2 = f32[4,1,512]{2,1,0:T(1,128)S(1)} all-gather(f32[1,1,512]{2,1,0:T(1,128)S(1)} %bitcast.439), channel_id=2, replica_groups=mesh['row'=8,'col'=4] {'col'}, dimensions={0}, use_global_device_ids=true | all-gather | bytes 10240 | tf_op jit(solution)/shard_map/all_gather | solution.py:77
  17.6 0.7 dynamic_slice.3
  18.3 3.2 %fusion.10 = bf16[64,8,8,128]{3,2,1,0:T(8,128)(2,1)S(1)} fusion(bf16[1024,1024]{1,0:T(8,128)(2,1)} %constant.151.clone, bf16[512,1024]{1,0:T(8,128)(2,1)} %param.7, f32[1024]{0:T(1024)S(1)} %dynamic_slice.3, f32[512]{0:T(512)S(1)} %add_rsqrt_fusion), kind=kOutput, calls=%fused_computation.19 | convolution fusion | flops 1076363264 | bytes 4200448 | tf_op jit(solution)/shard_map/dot_general | solution.py:81
  21.6 1.2 copy.26
  22.7 4.9 %all-to-all-start = ((bf16[512,8,128]{2,0,1:T(8,128)(2,1)}), bf16[512,8,128]{2,0,1:T(8,128)(2,1)S(1)}, u32[]{:S(2)}, u32[]{:S(2)}) async-start(bf16[512,8,128]{2,0,1:T(8,128)(2,1)} %bitcast.435), calls=%async_computation | async-start | bytes 2097152 | tf_op jit(solution)/shard_map/all_to_all | solution.py:82
  27.6 0.0 all-gather.5.cloned.1.call-start
  27.7 26.5 %all-to-all-done = bf16[512,8,128]{2,0,1:T(8,128)(2,1)S(1)} async-done(((bf16[512,8,128]{2,0,1:T(8,128)(2,1)}), bf16[512,8,128]{2,0,1:T(8,128)(2,1)S(1)}, u32[]{:S(2)}, u32[]{:S(2)}) %all-to-all-start) | async-done | bytes 1048608 | tf_op jit(solution)/shard_map/all_to_all | solution.py:82
  54.2 0.1 convert_bitcast_fusion
  54.3 0.0 copy-start.14
  54.3 0.0 copy-start.15
  54.3 0.0 copy-start.8
  54.4 0.0 copy-start.9
  54.4 0.3 fusion.23
  54.6 0.4 copy-done.14
  55.0 0.0 copy-done.15
  55.0 0.0 copy-start.6
  55.0 0.0 copy-start.7
  55.0 0.4 fusion.24
  55.4 0.0 copy-done.8
  55.4 0.0 copy-done.9
  55.4 0.0 copy-start.12
  55.5 0.0 copy-start.13
  55.5 0.4 fusion.25
  55.9 0.0 copy-done.6
  55.9 0.0 copy-done.7
  55.9 0.4 fusion.26
  56.3 0.0 copy-start.4
  56.3 0.0 copy-start.5
  56.3 0.0 copy-done.12
  56.3 0.0 copy-done.13
  56.3 0.3 fusion.27
  56.6 0.0 copy-start.2
  56.6 0.0 copy-start.3
  56.6 0.3 copy-done.4
  57.0 0.0 copy-done.5
  57.0 0.0 copy-start.10
  57.0 0.0 copy-start.11
  57.0 0.4 fusion.28
  57.4 0.0 copy-done.2
  57.4 0.0 copy-done.3
  57.4 0.4 fusion.29
  57.8 0.0 copy-done.10
  57.8 0.0 copy-done.11
  57.8 0.5 fusion.30
  58.3 0.0 copy-start.1
  58.3 0.3 fusion.17
  58.6 0.3 fusion.18
  58.9 0.3 fusion.19
  59.1 0.3 fusion.20
  59.4 0.3 fusion.21
  59.7 0.0 copy-start
  59.7 0.3 fusion.22
  60.0 0.0 copy-done.1
  60.0 0.7 fusion.50
  60.7 0.0 copy-done
  60.7 0.7 add_convert_fusion
  61.4 29.7 %all_to_all.18 = bf16[8,64,1024]{2,1,0:T(8,128)(2,1)} all-to-all(bf16[8,64,1024]{2,1,0:T(8,128)(2,1)S(1)} %bitcast.438), channel_id=1, replica_groups=mesh['row'=8,'col'=4] {'row'}, dimensions={0} | all-to-all | bytes 2097152 | tf_op jit(solution)/shard_map/all_to_all | solution.py:100
  91.1 0.0 all-gather.5.cloned.1.call-update
  91.2 14.8 %convolution_convert_fusion = bf16[1024,4,1024]{2,0,1:T(8,128)(2,1)} fusion(bf16[4,1024,1024]{2,1,0:T(8,128)(2,1)} %bitcast.440, s32[1024]{0:T(1024)S(1)} %get-tuple-element.30, bf16[1024]{0:T(1024)(128)(2,1)S(1)} %and_select_fusion, s32[1024]{0:T(1024)S(1)} %get-tuple-element.31), kind=kOutput, calls=%fused_computation | convolution fusion | flops 8598323200 | bytes 16787456 | tf_op jit(solution)/shard_map/sm,gme->gse/dot_general | solution.py:109
  106.0 35.9 %all-gather.5.cloned.1.call-done = bf16[32,64,1024]{2,1,0:T(8,128)(2,1)} async-done(((bf16[8,64,1024]{2,1,0:T(8,128)(2,1)}), bf16[32,64,1024]{2,1,0:T(8,128)(2,1)}) %all-gather.5.cloned.1.call-update) | async-done | bytes 4194320 | tf_op jit(solution)/shard_map/all_gather | solution.py:107
  141.8 3.5 %copy.24 = bf16[256,8,8,128]{3,2,1,0:T(8,128)(2,1)S(1)} copy(bf16[256,8,8,128]{3,1,2,0:T(8,128)(2,1)} %bitcast.436) | data formatting | bytes 8388608
  145.3 1.1 copy-done.16
  146.5 5.5 %fusion.11 = bf16[512,1024]{1,0:T(8,128)(2,1)} fusion(bf16[4,8,64,8,128]{4,3,2,1,0:T(8,128)(2,1)S(1)} %bitcast.437, bf16[4,8,128,1024,1]{3,2,4,1,0:T(8,128)(2,1)S(1)} %bitcast.441), kind=kOutput, calls=%fused_computation.20 | convolution fusion | flops 4295491584 | bytes 13631488 | tf_op jit(solution)/shard_map/gspql,gsle->pqe/dot_general | solution.py:115
  (6 shorter events, 0.1 us)
Async XLA Ops:
  22.7 31.5 %all-to-all-start = ((bf16[512,8,128]{2,0,1:T(8,128)(2,1)}), bf16[512,8,128]{2,0,1:T(8,128)(2,1)S(1)}, u32[]{:S(2)}, u32[]{:S(2)}) async-start(bf16[512,8,128]{2,0,1:T(8,128)(2,1)} %bitcast.435), calls=%async_computation | async-start | bytes 2097152 | tf_op jit(solution)/shard_map/all_to_all | solution.py:82
  27.6 114.2 %all-gather.5.cloned.1.call-start = ((), (), s32[]{:S(2)}) async-start(), calls=%async_computation.2 | async-start | bytes 5242880 | tf_op jit(solution)/shard_map/all_gather | solution.py:107
  54.3 0.7 copy-start.14
  54.3 0.7 copy-start.15
  54.3 1.1 copy-start.8
  54.4 1.1 copy-start.9
  55.0 0.8 copy-start.6
  55.0 0.8 copy-start.7
  55.4 0.9 copy-start.12
  55.5 0.9 copy-start.13
  56.3 0.7 copy-start.4
  56.3 0.7 copy-start.5
  56.6 0.8 copy-start.2
  56.6 0.8 copy-start.3
  57.0 0.8 copy-start.10
  57.0 0.8 copy-start.11
  58.3 1.6 %copy-start.1 = (bf16[512,512]{1,0:T(8,128)(2,1)S(1)}, bf16[512,512]{1,0:T(8,128)(2,1)}, u32[]{:S(2)}) copy-start(bf16[512,512]{1,0:T(8,128)(2,1)} %constant.187) | copy-start | bytes 1572868
  59.7 1.0 copy-start
  141.8 4.6 %copy-start.16 = (bf16[1024,4,1024]{2,0,1:T(8,128)(2,1)S(1)}, bf16[1024,4,1024]{2,0,1:T(8,128)(2,1)}, u32[]{:S(2)}) copy-start(bf16[1024,4,1024]{2,0,1:T(8,128)(2,1)} %convolution_convert_fusion) | copy-start | bytes 25165828
Sparse Core Ops, SparseCore 0:
  91.3 50.5 all-gather.4
